TPU v7x, 32 devices: a whole 2x2x4 slice. The times are simulated.
32 devices in a mesh: sp: 16 (over z, y, x), tp: 2 (over core).
Axes of the slice: x: 2, y: 2, z: 4, core: 2. Of those that a mesh axis runs over, the one named last changes fastest.
Arguments:
- query_one: bfloat16 [2048, 1024], P('sp', 'tp'), may hold values from -85 to 85
- key_one: bfloat16 [2048, 1024], P('sp', 'tp'), may hold values from -6.5 to 6.5
- query_two: bfloat16 [2048, 1024], P('sp', 'tp'), may hold values from -85 to 85
- key_two: bfloat16 [2048, 1024], P('sp', 'tp'), may hold values from -6.5 to 6.5
- values: bfloat16 [2048, 2048], P('sp', 'tp'), may hold values from -6 to 6
- mix_weight: float32 [8], P('tp'), may hold values from 0.3 to 0.8
- head_gain: float32 [256], replicated, may hold values from 0.1 to 1.9
- residual: bfloat16 [2048, 2048], P(('sp', 'tp')), may hold values from -6 to 6
- out_weight: bfloat16 [2048, 2048], P('tp'), may hold values from -0.125 to 0.125
- norm_gain: float32 [2048], replicated, may hold values from 0.1 to 1.9
- lift_weight: bfloat16 [2048, 5632], P('sp', 'tp'), may hold values from -0.125 to 0.125
- gate_weight: bfloat16 [2048, 5632], P('sp', 'tp'), may hold values from -0.125 to 0.125
- conv_taps: float32 [3, 5632], P(None, 'tp'), may hold values from -3 to 3
- down_weight: bfloat16 [5632, 2048], P('tp'), may hold values from -0.078125 to 0.078125
Outputs:
- layer_out: bfloat16 [2048, 2048], P(('sp', 'tp'))
All inputs are finite; a program needn't handle non-finite values.
Results may differ from a plain program's by a relative error of at most 0.015.
Values may be sent and summed in bfloat16 or wider, within the bound.
A program may use at most 128 MiB of HBM per device.

v0:
```python
import jax
import jax.numpy as jnp
from jax import lax
from jax.sharding import PartitionSpec as P

HD = 128
STRETCH = 64
WIDTH = 3
epsilon = 1e-06
masked_score = -1e30


def passed_along(block, axis, distance):
    devices = range(lax.axis_size(axis))
    route = [(i - distance, i) for i in devices if i - distance in devices]
    return lax.ppermute(block, axis, route)


def update_map(peak, total, acc, queries, keys, vals, visible):
    scores = jnp.einsum("thd,shd->hts", queries, keys, preferred_element_type=jnp.float32) * HD ** (
        -0.5
    )
    scores = jnp.where(visible[None], scores, masked_score)
    new_peak = jnp.maximum(peak, jnp.max(scores, axis=-1))
    weights = jnp.where(visible[None], jnp.exp(scores - new_peak[..., None]), 0.0)
    total = jnp.sum(weights, axis=-1)
    acc = jnp.einsum(
        "hts,she->hte", weights.astype(jnp.bfloat16), vals, preferred_element_type=jnp.float32
    )
    return (new_peak, total, acc)


def on_device(
    query_one,
    key_one,
    query_two,
    key_two,
    values,
    mix_weight,
    head_gain,
    residual,
    out_weight,
    norm_gain,
    lift_weight,
    gate_weight,
    conv_taps,
    down_weight,
):
    tok_local = query_one.shape[0]
    heads_local = mix_weight.shape[0]
    val_width = values.shape[1] // heads_local
    model_width = residual.shape[1]
    offset = lax.axis_index("sp") * tok_local
    q_pos = offset + lax.iota(jnp.int32, tok_local)
    q_one = query_one.reshape(tok_local, heads_local, HD)
    q_two = query_two.reshape(tok_local, heads_local, HD)
    start_peak = jnp.full((heads_local, tok_local), masked_score, jnp.float32)
    start_total = jnp.zeros((heads_local, tok_local), jnp.float32)
    start_acc = jnp.zeros((heads_local, tok_local, val_width), jnp.float32)
    initial = (start_peak, start_total, start_acc, start_peak, start_total, start_acc)
    first_keys = lax.all_gather(key_one, "sp", axis=0, tiled=True)
    second_keys = lax.all_gather(key_two, "sp", axis=0, tiled=True)
    piece_vals = lax.all_gather(values, "sp", axis=0, tiled=True)
    count = first_keys.shape[0]
    k_pos = lax.iota(jnp.int32, count)
    visible = k_pos[None, :] // STRETCH <= q_pos[:, None] // STRETCH
    first_keys = first_keys.reshape(count, heads_local, HD)
    second_keys = second_keys.reshape(count, heads_local, HD)
    piece_vals = piece_vals.reshape(count, heads_local, val_width)
    first = update_map(initial[0], initial[1], initial[2], q_one, first_keys, piece_vals, visible)
    second = update_map(initial[3], initial[4], initial[5], q_two, second_keys, piece_vals, visible)
    state = first + second
    mixed = (
        state[2] / state[1][..., None] - mix_weight[:, None, None] * state[5] / state[4][..., None]
    )
    head_out = (
        mixed * lax.rsqrt(jnp.mean(mixed * mixed, axis=-1, keepdims=True) + epsilon) * head_gain
    ).astype(jnp.bfloat16)
    out_heads = out_weight.reshape(heads_local, val_width, model_width)
    piece = head_out
    attended = lax.psum_scatter(
        jnp.einsum("hte,hed->td", piece, out_heads, preferred_element_type=jnp.float32).astype(
            jnp.bfloat16
        ),
        "tp",
        scatter_dimension=0,
        tiled=True,
    ).astype(jnp.float32)
    stream = residual.astype(jnp.float32) + attended
    normed = (
        stream * lax.rsqrt(jnp.mean(stream * stream, axis=-1, keepdims=True) + epsilon) * norm_gain
    ).astype(jnp.bfloat16)
    whole_rows = lax.all_gather(normed, "tp", axis=0, tiled=True)
    lift_pre = jnp.dot(
        whole_rows,
        lax.all_gather(lift_weight, "sp", axis=0, tiled=True),
        preferred_element_type=jnp.float32,
    )
    gate_pre = jnp.dot(
        whole_rows,
        lax.all_gather(gate_weight, "sp", axis=0, tiled=True),
        preferred_element_type=jnp.float32,
    )
    lifted = lift_pre.astype(jnp.bfloat16)
    gated = gate_pre.astype(jnp.bfloat16)
    prior = passed_along(gated[tok_local - (WIDTH - 1) :], "sp", 1)
    extended = jnp.concatenate([prior, gated], axis=0).astype(jnp.float32)
    conv = conv_taps[0] * extended[0:tok_local]
    for index in range(1, WIDTH):
        conv = conv + conv_taps[index] * extended[index : index + tok_local]
    hidden = (jax.nn.silu(conv) * lifted.astype(jnp.float32)).astype(jnp.bfloat16)
    piece = hidden
    mixer = lax.psum_scatter(
        jnp.dot(piece, down_weight, preferred_element_type=jnp.float32).astype(jnp.bfloat16),
        "tp",
        scatter_dimension=0,
        tiled=True,
    ).astype(jnp.float32)
    return (stream + mixer).astype(jnp.bfloat16)


def solution(mesh):
    return jax.shard_map(
        on_device,
        mesh=mesh,
        in_specs=(
            P("sp", "tp"),
            P("sp", "tp"),
            P("sp", "tp"),
            P("sp", "tp"),
            P("sp", "tp"),
            P("tp"),
            P(),
            P(("sp", "tp"), None),
            P("tp", None),
            P(),
            P("sp", "tp"),
            P("sp", "tp"),
            P(None, "tp"),
            P("tp", None),
        ),
        out_specs=P(("sp", "tp"), None),
        check_vma=False,
    )
```

profile of v0, /device:TPU:0, one launch (start us, length us, event | category | flops | bytes accessed | tf_op | source)
XLA Modules:
  0.0 559.7 jit_solution(8064380941577082344)
XLA Ops:
  6.5 1.7 copy.17
  8.3 1.7 copy.22
  10.0 1.8 copy.20
  12.2 63.6 %all-gather.6.cloned.1.call-done = bf16[2048,512]{0,1:T(8,128)(2,1)} async-done(((bf16[128,512]{0,1:T(8,128)(2,1)}), bf16[2048,512]{0,1:T(8,128)(2,1)}) %all-gather.6.cloned.1.call-update) | async-done | bytes 2097168 | tf_op jit(solution)/shard_map/all_gather | solution.py:61
  75.7 4.7 fusion
  80.4 59.2 %all-gather.10.cloned.1.call-done = bf16[2048,512]{0,1:T(8,128)(2,1)} async-done(((bf16[128,512]{0,1:T(8,128)(2,1)}), bf16[2048,512]{0,1:T(8,128)(2,1)}) %all-gather.10.cloned.1.call-update) | async-done | bytes 2097168 | tf_op jit(solution)/shard_map/all_gather | solution.py:62
  139.6 5.1 fusion.5
  144.7 1.9 copy-done.3
  146.6 1.3 fusion.7
  147.9 81.3 %all-gather.8.cloned.1.call-done = bf16[2048,1024]{0,1:T(8,128)(2,1)} async-done(((bf16[128,1024]{0,1:T(8,128)(2,1)}), bf16[2048,1024]{0,1:T(8,128)(2,1)}) %all-gather.8.cloned.1.call-update) | async-done | bytes 4194320 | tf_op jit(solution)/shard_map/all_gather | solution.py:63
  229.2 5.5 fusion.35
  235.2 2.1 multiply_reduce_fusion.1
  237.4 1.6 fusion.9
  240.2 5.0 reduce-scatter.3.cloned.1.call-done
  245.2 1.1 multiply_reduce_fusion
  247.5 2.2 all_gather.21
  249.6 140.8 %all-gather.12.cloned.1.call-done = bf16[2048,2816]{1,0:T(8,128)(2,1)} async-done(((bf16[128,2816]{1,0:T(8,128)(2,1)}), bf16[2048,2816]{1,0:T(8,128)(2,1)}) %all-gather.12.cloned.1.call-update) | async-done | bytes 11534352 | tf_op jit(solution)/shard_map/all_gather | solution.py:101
  390.4 5.9 %convolution_convert_fusion.1 = bf16[128,2816]{1,0:T(8,128)(2,1)S(1)} fusion(bf16[128,2048]{1,0:T(8,128)(2,1)S(1)} %all_gather.21, bf16[2048,2816]{1,0:T(8,128)(2,1)} %all-gather.12.cloned.1.call-done), kind=kOutput, calls=%fused_computation.10 | convolution fusion | flops 1476755456 | bytes 12779520 | tf_op jit(solution)/shard_map/dot_general | solution.py:99
  396.4 3.4 collective-permute-start
  399.9 1.1 collective-permute-done
  401.1 131.5 %all-gather.14.cloned.1.call-done = bf16[2048,2816]{1,0:T(8,128)(2,1)} async-done(((bf16[128,2816]{1,0:T(8,128)(2,1)}), bf16[2048,2816]{1,0:T(8,128)(2,1)}) %all-gather.14.cloned.1.call-update) | async-done | bytes 11534352 | tf_op jit(solution)/shard_map/all_gather | solution.py:96
  532.7 12.1 %convolution_convert_fusion.2 = bf16[128,2048]{1,0:T(8,128)(2,1)} fusion(bf16[2816,2048]{1,0:T(8,128)(2,1)} %param.27, bf16[128,2048]{1,0:T(8,128)(2,1)S(1)} %all_gather.21, bf16[2048,2816]{1,0:T(8,128)(2,1)} %all-gather.14.cloned.1.call-done, f32[130,2816]{1,0:T(8,128)S(1)} %maximum_convert_fusion, f32[2816]{0:T(1024)S(1)} %get-tuple-element.8, ...), kind=kOutput, calls=%fused_computation.17 | convolution fusion | flops 2957737984 | bytes 28479488 | tf_op jit(solution)/shard_map/dot_general | solution.py:114
  544.8 6.3 %reduce-scatter.5.cloned.1.call-done = bf16[64,2048]{1,0:T(8,128)(2,1)} async-done(((bf16[128,2048]{1,0:T(8,128)(2,1)}), bf16[64,2048]{1,0:T(8,128)(2,1)}) %reduce-scatter.5.cloned.1.call-update) | async-done | bytes 262160 | tf_op jit(solution)/shard_map/reduce_scatter | solution.py:113
  551.1 1.7 add_convert_fusion
  (46 shorter events, 3.5 us)
Async XLA Ops:
  6.5 133.1 %copy-start = (bf16[128,512]{1,0:T(8,128)(2,1)S(1)}, bf16[128,512]{1,0:T(8,128)(2,1)}, u32[]{:S(2)}) copy-start(bf16[128,512]{1,0:T(8,128)(2,1)} %param.16) | copy-start | bytes 393220
  6.5 69.2 %all-gather.6.cloned.1.call-start = ((), (), s32[]{:S(2)}) async-start(), calls=%async_computation.2 | async-start | bytes 2228224 | tf_op jit(solution)/shard_map/all_gather | solution.py:61
  8.3 131.3 %all-gather.10.cloned.1.call-start = ((), (), s32[]{:S(2)}) async-start(), calls=%async_computation.4 | async-start | bytes 2228224 | tf_op jit(solution)/shard_map/all_gather | solution.py:62
  10.0 219.2 %all-gather.8.cloned.1.call-start = ((), (), s32[]{:S(2)}) async-start(), calls=%async_computation.3 | async-start | bytes 4456448 | tf_op jit(solution)/shard_map/all_gather | solution.py:63
  11.9 233.4 %reduce-scatter.3.cloned.1.call-start = ((), (), s32[]{:S(2)}) async-start(), calls=%async_computation.5 | async-start | bytes 786432 | tf_op jit(solution)/shard_map/reduce_scatter | solution.py:81
  144.7 1.9 copy-start.3
  144.7 84.5 %copy-start.10 = (f32[4]{0:T(128)S(1)}, f32[4]{0:T(128)}, u32[]{:S(2)}) copy-start(f32[4]{0:T(128)} %param.19) | copy-start | bytes 52
  229.2 5.5 copy-start.2
  229.2 5.9 %copy-start.9 = (bf16[2048,1024]{0,1:T(8,128)(2,1)S(1)}, bf16[2048,1024]{0,1:T(8,128)(2,1)}, u32[]{:S(2)}) copy-start(bf16[2048,1024]{0,1:T(8,128)(2,1)} %all-gather.8.cloned.1.call-done) | copy-start | bytes 12582916
  235.2 2.2 copy-start.1
  235.2 2.2 copy-start.8
  237.3 7.9 %copy-start.4 = (bf16[64,2048]{1,0:T(8,128)(2,1)S(1)}, bf16[64,2048]{1,0:T(8,128)(2,1)}, u32[]{:S(2)}) copy-start(bf16[64,2048]{1,0:T(8,128)(2,1)} %param.21) | copy-start | bytes 786436
  237.4 9.0 %copy-start.7 = (f32[2048]{0:T(1024)S(1)}, f32[2048]{0:T(1024)}, u32[]{:S(2)}) copy-start(f32[2048]{0:T(1024)} %param.23) | copy-start | bytes 24580
  239.0 151.4 %all-gather.12.cloned.1.call-start = ((), (), s32[]{:S(2)}) async-start(), calls=%async_computation.6 | async-start | bytes 12255232 | tf_op jit(solution)/shard_map/all_gather | solution.py:101
  239.6 293.1 %all-gather.14.cloned.1.call-start = ((), (), s32[]{:S(2)}) async-start(), calls=%async_computation.7 | async-start | bytes 12255232 | tf_op jit(solution)/shard_map/all_gather | solution.py:96
  240.1 310.9 %reduce-scatter.5.cloned.1.call-start = ((), (), s32[]{:S(2)}) async-start(), calls=%async_computation.8 | async-start | bytes 786432 | tf_op jit(solution)/shard_map/reduce_scatter | solution.py:113
  249.6 150.1 %copy-start.6 = (f32[3,2816]{1,0:T(4,128)S(1)}, f32[3,2816]{1,0:T(4,128)}, u32[]{:S(2)}) copy-start(f32[3,2816]{1,0:T(4,128)} %param.26) | copy-start | bytes 101380
  396.4 4.6 collective-permute-start
  532.7 18.4 %copy-start.5 = (bf16[64,2048]{1,0:T(8,128)(2,1)S(1)}, bf16[64,2048]{1,0:T(8,128)(2,1)}, u32[]{:S(2)}) copy-start(bf16[64,2048]{1,0:T(8,128)(2,1)} %reduce-scatter.3.cloned.1.call-done) | copy-start | bytes 786436
Sparse Core Ops, SparseCore 0:
  10.0 65.6 all-gather.5
  78.4 61.1 all-gather.9
  142.3 86.8 all-gather.7
  239.1 6.0 reduce-scatter.2
  247.8 142.5 all-gather.11
  393.0 139.5 all-gather.13
  544.9 6.0 reduce-scatter.4
where the time goes:
time: 560 us
  waiting for transfers between devices  490 us (88%)
  matrix products  37 us (7%)
  between operations  13.6 us (2%)
  local copies, waits for them, and re-layouts  7.68 us (1%)
  other arithmetic  5.62 us (1%)
    all_gather x1, waiting for transfers between devices, on_device(): lax.all_gather(gate_weight, 'sp', axis=0, tiled=True)  141 us
    all_gather x1, waiting for transfers between devices, on_device(): lax.all_gather(lift_weight, 'sp', axis=0, tiled=True)  132 us
    all_gather x1, waiting for transfers between devices, on_device(): piece_vals = lax.all_gather(values, 'sp', axis=0, tiled=True)  81.3 us
    all_gather x1, waiting for transfers between devices, on_device(): first_keys = lax.all_gather(key_one, 'sp', axis=0, tiled=True)  63.6 us
    all_gather x1, waiting for transfers between devices, on_device(): second_keys = lax.all_gather(key_two, 'sp', axis=0, tiled=True)  59.2 us
    dot_general x1, matrix products, on_device(): jnp.dot(piece, down_weight, preferred_element_type=jnp.float32)  12.1 us
  transfers between devices with their start and end apart: 8, of which 8 were waited for; matrix products, arithmetic and copies ran while one was open for 4% of the time, Pallas kernels for 0%

commit v1 on v0

--- a/solution.py
+++ b/solution.py
@@ -59,7 +59,12 @@
     start_acc = jnp.zeros((heads_local, tok_local, val_width), jnp.float32)
     initial = (start_peak, start_total, start_acc, start_peak, start_total, start_acc)
     first_keys = lax.all_gather(key_one, "sp", axis=0, tiled=True)
-    second_keys = lax.all_gather(key_two, "sp", axis=0, tiled=True)
+    ring = [key_two]
+    for hop in range(15):
+        ring.append(lax.ppermute(ring[-1], "sp", [(dev, (dev + 1) % 16) for dev in range(16)]))
+    second_keys = jnp.roll(
+        jnp.concatenate(ring[::-1], axis=0), (lax.axis_index("sp") + 1) * ring[0].shape[0], axis=0
+    )
     piece_vals = lax.all_gather(values, "sp", axis=0, tiled=True)
     count = first_keys.shape[0]
     k_pos = lax.iota(jnp.int32, count)

time: 560 us -> 515 us (0.920)
  waiting for transfers between devices: 490 us -> 446 us
    ppermute x0 -> x15, waiting for transfers between devices: none -> 143 us  [on_device(): lax.ppermute(ring[-1], 'sp', [(dev, (dev + 1) % 16) for dev in range(16)])]
    all_gather x1, waiting for transfers between devices: 81.3 us -> 15.9 us  [on_device(): piece_vals = lax.all_gather(values, 'sp', axis=0, tiled=True)]
    all_gather x1, waiting for transfers between devices: 63.6 us -> 0.02 us  [on_device(): first_keys = lax.all_gather(key_one, 'sp', axis=0, tiled=True)]
    all_gather x1 -> x0, waiting for transfers between devices: 59.2 us -> none  [on_device(): second_keys = lax.all_gather(key_two, 'sp', axis=0, tiled=True)]
  transfers between devices with their start and end apart: 8 -> 22, of which waited for: 8 -> 21; matrix products, arithmetic and copies ran while one was open for 4% -> 4% of each run, Pallas kernels for 0% -> 0%
where the time goes in v1:
time: 515 us
  waiting for transfers between devices  446 us (87%)
  matrix products  32.3 us (6%)
  between operations  14 us (3%)
  local copies, waits for them, and re-layouts  8.53 us (2%)
  starting transfers between devices  6.43 us (1%)
  other arithmetic  5.62 us (1%)
    ppermute x15, waiting for transfers between devices, on_device(): lax.ppermute(ring[-1], 'sp', [(dev, (dev + 1) % 16) for dev in range(16)])  143 us
    all_gather x1, waiting for transfers between devices, on_device(): lax.all_gather(gate_weight, 'sp', axis=0, tiled=True)  141 us
    all_gather x1, waiting for transfers between devices, on_device(): lax.all_gather(lift_weight, 'sp', axis=0, tiled=True)  132 us
    all_gather x1, waiting for transfers between devices, on_device(): piece_vals = lax.all_gather(values, 'sp', axis=0, tiled=True)  15.9 us
    dot_general x1, matrix products, on_device(): jnp.dot(piece, down_weight, preferred_element_type=jnp.float32)  12.2 us
  transfers between devices with their start and end apart: 22, of which 21 were waited for; matrix products, arithmetic and copies ran while one was open for 4% of the time, Pallas kernels for 0%

profile of v1, /device:TPU:0, one launch (start us, length us, event | category | flops | bytes accessed | tf_op | source)
XLA Modules:
  0.0 514.7 jit_solution(15980985146507221859)
XLA Ops:
  12.4 7.5 %collective-permute-done = bf16[128,512]{0,1:T(8,128)(2,1)S(1)} collective-permute-done((bf16[128,512]{0,1:T(8,128)(2,1)S(1)}, bf16[128,512]{0,1:T(8,128)(2,1)S(1)}, u32[]{:S(2)}, u32[]{:S(2)}) %collective-permute-start) | collective-permute-done | bytes 131104 | tf_op jit(solution)/shard_map/ppermute | solution.py:64
  19.9 8.6 %collective-permute-done.1 = bf16[128,512]{0,1:T(8,128)(2,1)S(1)} collective-permute-done((bf16[128,512]{0,1:T(8,128)(2,1)S(1)}, bf16[128,512]{0,1:T(8,128)(2,1)S(1)}, u32[]{:S(2)}, u32[]{:S(2)}) %collective-permute-start.1) | collective-permute-done | bytes 131104 | tf_op jit(solution)/shard_map/ppermute | solution.py:64
  28.4 8.6 %collective-permute-done.2 = bf16[128,512]{0,1:T(8,128)(2,1)S(1)} collective-permute-done((bf16[128,512]{0,1:T(8,128)(2,1)S(1)}, bf16[128,512]{0,1:T(8,128)(2,1)S(1)}, u32[]{:S(2)}, u32[]{:S(2)}) %collective-permute-start.2) | collective-permute-done | bytes 131104 | tf_op jit(solution)/shard_map/ppermute | solution.py:64
  38.9 7.1 %collective-permute-done.3 = bf16[128,512]{0,1:T(8,128)(2,1)S(1)} collective-permute-done((bf16[128,512]{0,1:T(8,128)(2,1)S(1)}, bf16[128,512]{0,1:T(8,128)(2,1)S(1)}, u32[]{:S(2)}, u32[]{:S(2)}) %collective-permute-start.3) | collective-permute-done | bytes 131104 | tf_op jit(solution)/shard_map/ppermute | solution.py:64
  45.9 8.7 %collective-permute-done.4 = bf16[128,512]{0,1:T(8,128)(2,1)S(1)} collective-permute-done((bf16[128,512]{0,1:T(8,128)(2,1)S(1)}, bf16[128,512]{0,1:T(8,128)(2,1)S(1)}, u32[]{:S(2)}, u32[]{:S(2)}) %collective-permute-start.4) | collective-permute-done | bytes 131104 | tf_op jit(solution)/shard_map/ppermute | solution.py:64
  54.7 9.1 %collective-permute-done.5 = bf16[128,512]{0,1:T(8,128)(2,1)S(1)} collective-permute-done((bf16[128,512]{0,1:T(8,128)(2,1)S(1)}, bf16[128,512]{0,1:T(8,128)(2,1)S(1)}, u32[]{:S(2)}, u32[]{:S(2)}) %collective-permute-start.5) | collective-permute-done | bytes 131104 | tf_op jit(solution)/shard_map/ppermute | solution.py:64
  63.8 10.8 %collective-permute-done.6 = bf16[128,512]{0,1:T(8,128)(2,1)S(1)} collective-permute-done((bf16[128,512]{0,1:T(8,128)(2,1)S(1)}, bf16[128,512]{0,1:T(8,128)(2,1)S(1)}, u32[]{:S(2)}, u32[]{:S(2)}) %collective-permute-start.6) | collective-permute-done | bytes 131104 | tf_op jit(solution)/shard_map/ppermute | solution.py:64
  74.6 11.6 %collective-permute-done.7 = bf16[128,512]{0,1:T(8,128)(2,1)S(1)} collective-permute-done((bf16[128,512]{0,1:T(8,128)(2,1)S(1)}, bf16[128,512]{0,1:T(8,128)(2,1)S(1)}, u32[]{:S(2)}, u32[]{:S(2)}) %collective-permute-start.7) | collective-permute-done | bytes 131104 | tf_op jit(solution)/shard_map/ppermute | solution.py:64
  86.2 8.6 %collective-permute-done.8 = bf16[128,512]{0,1:T(8,128)(2,1)S(1)} collective-permute-done((bf16[128,512]{0,1:T(8,128)(2,1)S(1)}, bf16[128,512]{0,1:T(8,128)(2,1)S(1)}, u32[]{:S(2)}, u32[]{:S(2)}) %collective-permute-start.8) | collective-permute-done | bytes 131104 | tf_op jit(solution)/shard_map/ppermute | solution.py:64
  94.8 9.8 %collective-permute-done.9 = bf16[128,512]{0,1:T(8,128)(2,1)S(1)} collective-permute-done((bf16[128,512]{0,1:T(8,128)(2,1)S(1)}, bf16[128,512]{0,1:T(8,128)(2,1)S(1)}, u32[]{:S(2)}, u32[]{:S(2)}) %collective-permute-start.9) | collective-permute-done | bytes 131104 | tf_op jit(solution)/shard_map/ppermute | solution.py:64
  104.6 9.1 %collective-permute-done.10 = bf16[128,512]{0,1:T(8,128)(2,1)S(1)} collective-permute-done((bf16[128,512]{0,1:T(8,128)(2,1)S(1)}, bf16[128,512]{0,1:T(8,128)(2,1)S(1)}, u32[]{:S(2)}, u32[]{:S(2)}) %collective-permute-start.10) | collective-permute-done | bytes 131104 | tf_op jit(solution)/shard_map/ppermute | solution.py:64
  113.6 12.2 %collective-permute-done.11 = bf16[128,512]{0,1:T(8,128)(2,1)S(1)} collective-permute-done((bf16[128,512]{0,1:T(8,128)(2,1)S(1)}, bf16[128,512]{0,1:T(8,128)(2,1)S(1)}, u32[]{:S(2)}, u32[]{:S(2)}) %collective-permute-start.11) | collective-permute-done | bytes 131104 | tf_op jit(solution)/shard_map/ppermute | solution.py:64
  125.8 11.9 %collective-permute-done.12 = bf16[128,512]{0,1:T(8,128)(2,1)S(1)} collective-permute-done((bf16[128,512]{0,1:T(8,128)(2,1)S(1)}, bf16[128,512]{0,1:T(8,128)(2,1)S(1)}, u32[]{:S(2)}, u32[]{:S(2)}) %collective-permute-start.12) | collective-permute-done | bytes 131104 | tf_op jit(solution)/shard_map/ppermute | solution.py:64
  137.7 8.5 %collective-permute-done.13 = bf16[128,512]{0,1:T(8,128)(2,1)S(1)} collective-permute-done((bf16[128,512]{0,1:T(8,128)(2,1)S(1)}, bf16[128,512]{0,1:T(8,128)(2,1)S(1)}, u32[]{:S(2)}, u32[]{:S(2)}) %collective-permute-start.13) | collective-permute-done | bytes 131104 | tf_op jit(solution)/shard_map/ppermute | solution.py:64
  146.5 11.3 %collective-permute-done.14 = bf16[128,512]{0,1:T(8,128)(2,1)S(1)} collective-permute-done((bf16[128,512]{0,1:T(8,128)(2,1)S(1)}, bf16[128,512]{0,1:T(8,128)(2,1)S(1)}, u32[]{:S(2)}, u32[]{:S(2)}) %collective-permute-start.14) | collective-permute-done | bytes 131104 | tf_op jit(solution)/shard_map/ppermute | solution.py:64
  167.8 15.9 %all-gather.7.cloned.1.call-done = bf16[2048,1024]{0,1:T(8,128)(2,1)} async-done(((bf16[128,1024]{0,1:T(8,128)(2,1)}), bf16[2048,1024]{0,1:T(8,128)(2,1)}) %all-gather.7.cloned.1.call-update) | async-done | bytes 4194320 | tf_op jit(solution)/shard_map/all_gather | solution.py:68
  183.7 5.5 %fusion.35 = f32[4,128,256]{2,1,0:T(8,128)S(1)} fusion(bf16[2048,4,256]{0,2,1:T(8,128)(2,1)} %bitcast.54, f32[4,2048,128]{1,2,0:T(8,128)} %copy-done.5, f32[4,128]{1,0:T(4,128)S(1)} %broadcast_maximum_fusion, pred[128,2048]{1,0:T(8,128)(4,1)S(1)} %broadcast_compare_fusion, f32[4,128]{1,0:T(4,128)S(1)} %fusion.7, f32[4]{0:T(128)S(1)} %copy-done.13), kind=kOutput, calls=%fused_computation.38 | convolution fusion | flops 542375936 | bytes 9179152 | tf_op jit(solution)/shard_map/hts,she->hte/dot_general | solution.py:27
  194.6 5.6 %reduce-scatter.3.cloned.1.call-done = bf16[64,2048]{1,0:T(8,128)(2,1)} async-done(((bf16[128,2048]{1,0:T(8,128)(2,1)}), bf16[64,2048]{1,0:T(8,128)(2,1)}) %reduce-scatter.3.cloned.1.call-update) | async-done | bytes 262160 | tf_op jit(solution)/shard_map/reduce_scatter | solution.py:86
  204.9 140.6 %all-gather.9.cloned.1.call-done = bf16[2048,2816]{1,0:T(8,128)(2,1)} async-done(((bf16[128,2816]{1,0:T(8,128)(2,1)}), bf16[2048,2816]{1,0:T(8,128)(2,1)}) %all-gather.9.cloned.1.call-update) | async-done | bytes 11534352 | tf_op jit(solution)/shard_map/all_gather | solution.py:106
  345.5 6.0 %convolution_convert_fusion.1 = bf16[128,2816]{1,0:T(8,128)(2,1)S(1)} fusion(bf16[128,2048]{1,0:T(8,128)(2,1)S(1)} %all_gather.17, bf16[2048,2816]{1,0:T(8,128)(2,1)} %all-gather.9.cloned.1.call-done), kind=kOutput, calls=%fused_computation.10 | convolution fusion | flops 1476755456 | bytes 12779520 | tf_op jit(solution)/shard_map/dot_general | solution.py:104
  351.4 3.2 collective-permute-start.15
  356.2 131.5 %all-gather.11.cloned.1.call-done = bf16[2048,2816]{1,0:T(8,128)(2,1)} async-done(((bf16[128,2816]{1,0:T(8,128)(2,1)}), bf16[2048,2816]{1,0:T(8,128)(2,1)}) %all-gather.11.cloned.1.call-update) | async-done | bytes 11534352 | tf_op jit(solution)/shard_map/all_gather | solution.py:101
  487.7 12.2 %convolution_convert_fusion.2 = bf16[128,2048]{1,0:T(8,128)(2,1)} fusion(bf16[2816,2048]{1,0:T(8,128)(2,1)} %param.27, bf16[128,2048]{1,0:T(8,128)(2,1)S(1)} %all_gather.17, bf16[2048,2816]{1,0:T(8,128)(2,1)} %all-gather.11.cloned.1.call-done, f32[130,2816]{1,0:T(8,128)S(1)} %maximum_convert_fusion, f32[2816]{0:T(1024)S(1)} %get-tuple-element.8, ...), kind=kOutput, calls=%fused_computation.17 | convolution fusion | flops 2957737984 | bytes 28479488 | tf_op jit(solution)/shard_map/dot_general | solution.py:119
  499.9 6.3 %reduce-scatter.5.cloned.1.call-done = bf16[64,2048]{1,0:T(8,128)(2,1)} async-done(((bf16[128,2048]{1,0:T(8,128)(2,1)}), bf16[64,2048]{1,0:T(8,128)(2,1)}) %reduce-scatter.5.cloned.1.call-update) | async-done | bytes 262160 | tf_op jit(solution)/shard_map/reduce_scatter | solution.py:118
  (112 shorter events, 30.9 us)
Async XLA Ops:
  6.5 155.7 %copy-start = (bf16[128,512]{1,0:T(8,128)(2,1)S(1)}, bf16[128,512]{1,0:T(8,128)(2,1)}, u32[]{:S(2)}) copy-start(bf16[128,512]{1,0:T(8,128)(2,1)} %param.16) | copy-start | bytes 393220
  6.5 152.9 %all-gather.5.cloned.1.call-start = ((), (), s32[]{:S(2)}) async-start(), calls=%async_computation.2 | async-start | bytes 2228224 | tf_op jit(solution)/shard_map/all_gather | solution.py:61
  8.3 175.4 %all-gather.7.cloned.1.call-start = ((), (), s32[]{:S(2)}) async-start(), calls=%async_computation.3 | async-start | bytes 4456448 | tf_op jit(solution)/shard_map/all_gather | solution.py:68
  9.3 10.5 %collective-permute-start = (bf16[128,512]{0,1:T(8,128)(2,1)S(1)}, bf16[128,512]{0,1:T(8,128)(2,1)S(1)}, u32[]{:S(2)}, u32[]{:S(2)}) collective-permute-start(bf16[128,512]{0,1:T(8,128)(2,1)S(1)} %copy.23), channel_id=1, source_target_pairs={{0,2},{2,4},{4,6},{6,8},{8,10},{10,12},{12,14},{14,16},{16,18},{18... | collective-permute-start | bytes 393224 | tf_op jit(solution)/shard_map/ppermute | solution.py:64
  19.8 8.6 %collective-permute-start.1 = (bf16[128,512]{0,1:T(8,128)(2,1)S(1)}, bf16[128,512]{0,1:T(8,128)(2,1)S(1)}, u32[]{:S(2)}, u32[]{:S(2)}) collective-permute-start(bf16[128,512]{0,1:T(8,128)(2,1)S(1)} %collective-permute-done), channel_id=1, source_target_pairs={{0,2},{2,4},{4,6},{6,8},{8,10},{10,12},{12,14},{14,16},{16,18},{18... | collective-permute-start | bytes 393224 | tf_op jit(solution)/shard_map/ppermute | solution.py:64
  28.4 8.6 %collective-permute-start.2 = (bf16[128,512]{0,1:T(8,128)(2,1)S(1)}, bf16[128,512]{0,1:T(8,128)(2,1)S(1)}, u32[]{:S(2)}, u32[]{:S(2)}) collective-permute-start(bf16[128,512]{0,1:T(8,128)(2,1)S(1)} %collective-permute-done.1), channel_id=1, source_target_pairs={{0,2},{2,4},{4,6},{6,8},{8,10},{10,12},{12,14},{14,16},{16,18},{18... | collective-permute-start | bytes 393224 | tf_op jit(solution)/shard_map/ppermute | solution.py:64
  37.0 8.9 %collective-permute-start.3 = (bf16[128,512]{0,1:T(8,128)(2,1)S(1)}, bf16[128,512]{0,1:T(8,128)(2,1)S(1)}, u32[]{:S(2)}, u32[]{:S(2)}) collective-permute-start(bf16[128,512]{0,1:T(8,128)(2,1)S(1)} %collective-permute-done.2), channel_id=1, source_target_pairs={{0,2},{2,4},{4,6},{6,8},{8,10},{10,12},{12,14},{14,16},{16,18},{18... | collective-permute-start | bytes 393224 | tf_op jit(solution)/shard_map/ppermute | solution.py:64
  38.8 161.5 %reduce-scatter.3.cloned.1.call-start = ((), (), s32[]{:S(2)}) async-start(), calls=%async_computation.4 | async-start | bytes 786432 | tf_op jit(solution)/shard_map/reduce_scatter | solution.py:86
  45.9 8.7 %collective-permute-start.4 = (bf16[128,512]{0,1:T(8,128)(2,1)S(1)}, bf16[128,512]{0,1:T(8,128)(2,1)S(1)}, u32[]{:S(2)}, u32[]{:S(2)}) collective-permute-start(bf16[128,512]{0,1:T(8,128)(2,1)S(1)} %collective-permute-done.3), channel_id=1, source_target_pairs={{0,2},{2,4},{4,6},{6,8},{8,10},{10,12},{12,14},{14,16},{16,18},{18... | collective-permute-start | bytes 393224 | tf_op jit(solution)/shard_map/ppermute | solution.py:64
  54.7 9.1 %collective-permute-start.5 = (bf16[128,512]{0,1:T(8,128)(2,1)S(1)}, bf16[128,512]{0,1:T(8,128)(2,1)S(1)}, u32[]{:S(2)}, u32[]{:S(2)}) collective-permute-start(bf16[128,512]{0,1:T(8,128)(2,1)S(1)} %collective-permute-done.4), channel_id=1, source_target_pairs={{0,2},{2,4},{4,6},{6,8},{8,10},{10,12},{12,14},{14,16},{16,18},{18... | collective-permute-start | bytes 393224 | tf_op jit(solution)/shard_map/ppermute | solution.py:64
  63.8 10.9 %collective-permute-start.6 = (bf16[128,512]{0,1:T(8,128)(2,1)S(1)}, bf16[128,512]{0,1:T(8,128)(2,1)S(1)}, u32[]{:S(2)}, u32[]{:S(2)}) collective-permute-start(bf16[128,512]{0,1:T(8,128)(2,1)S(1)} %collective-permute-done.5), channel_id=1, source_target_pairs={{0,2},{2,4},{4,6},{6,8},{8,10},{10,12},{12,14},{14,16},{16,18},{18... | collective-permute-start | bytes 393224 | tf_op jit(solution)/shard_map/ppermute | solution.py:64
  74.6 11.6 %collective-permute-start.7 = (bf16[128,512]{0,1:T(8,128)(2,1)S(1)}, bf16[128,512]{0,1:T(8,128)(2,1)S(1)}, u32[]{:S(2)}, u32[]{:S(2)}) collective-permute-start(bf16[128,512]{0,1:T(8,128)(2,1)S(1)} %collective-permute-done.6), channel_id=1, source_target_pairs={{0,2},{2,4},{4,6},{6,8},{8,10},{10,12},{12,14},{14,16},{16,18},{18... | collective-permute-start | bytes 393224 | tf_op jit(solution)/shard_map/ppermute | solution.py:64
  86.2 8.6 %collective-permute-start.8 = (bf16[128,512]{0,1:T(8,128)(2,1)S(1)}, bf16[128,512]{0,1:T(8,128)(2,1)S(1)}, u32[]{:S(2)}, u32[]{:S(2)}) collective-permute-start(bf16[128,512]{0,1:T(8,128)(2,1)S(1)} %collective-permute-done.7), channel_id=1, source_target_pairs={{0,2},{2,4},{4,6},{6,8},{8,10},{10,12},{12,14},{14,16},{16,18},{18... | collective-permute-start | bytes 393224 | tf_op jit(solution)/shard_map/ppermute | solution.py:64
  94.8 9.8 %collective-permute-start.9 = (bf16[128,512]{0,1:T(8,128)(2,1)S(1)}, bf16[128,512]{0,1:T(8,128)(2,1)S(1)}, u32[]{:S(2)}, u32[]{:S(2)}) collective-permute-start(bf16[128,512]{0,1:T(8,128)(2,1)S(1)} %collective-permute-done.8), channel_id=1, source_target_pairs={{0,2},{2,4},{4,6},{6,8},{8,10},{10,12},{12,14},{14,16},{16,18},{18... | collective-permute-start | bytes 393224 | tf_op jit(solution)/shard_map/ppermute | solution.py:64
  104.6 9.1 %collective-permute-start.10 = (bf16[128,512]{0,1:T(8,128)(2,1)S(1)}, bf16[128,512]{0,1:T(8,128)(2,1)S(1)}, u32[]{:S(2)}, u32[]{:S(2)}) collective-permute-start(bf16[128,512]{0,1:T(8,128)(2,1)S(1)} %collective-permute-done.9), channel_id=1, source_target_pairs={{0,2},{2,4},{4,6},{6,8},{8,10},{10,12},{12,14},{14,16},{16,18},{18... | collective-permute-start | bytes 393224 | tf_op jit(solution)/shard_map/ppermute | solution.py:64
  113.6 12.2 %collective-permute-start.11 = (bf16[128,512]{0,1:T(8,128)(2,1)S(1)}, bf16[128,512]{0,1:T(8,128)(2,1)S(1)}, u32[]{:S(2)}, u32[]{:S(2)}) collective-permute-start(bf16[128,512]{0,1:T(8,128)(2,1)S(1)} %collective-permute-done.10), channel_id=1, source_target_pairs={{0,2},{2,4},{4,6},{6,8},{8,10},{10,12},{12,14},{14,16},{16,18},{18... | collective-permute-start | bytes 393224 | tf_op jit(solution)/shard_map/ppermute | solution.py:64
  125.8 11.9 %collective-permute-start.12 = (bf16[128,512]{0,1:T(8,128)(2,1)S(1)}, bf16[128,512]{0,1:T(8,128)(2,1)S(1)}, u32[]{:S(2)}, u32[]{:S(2)}) collective-permute-start(bf16[128,512]{0,1:T(8,128)(2,1)S(1)} %collective-permute-done.11), channel_id=1, source_target_pairs={{0,2},{2,4},{4,6},{6,8},{8,10},{10,12},{12,14},{14,16},{16,18},{18... | collective-permute-start | bytes 393224 | tf_op jit(solution)/shard_map/ppermute | solution.py:64
  137.7 8.6 %collective-permute-start.13 = (bf16[128,512]{0,1:T(8,128)(2,1)S(1)}, bf16[128,512]{0,1:T(8,128)(2,1)S(1)}, u32[]{:S(2)}, u32[]{:S(2)}) collective-permute-start(bf16[128,512]{0,1:T(8,128)(2,1)S(1)} %collective-permute-done.12), channel_id=1, source_target_pairs={{0,2},{2,4},{4,6},{6,8},{8,10},{10,12},{12,14},{14,16},{16,18},{18... | collective-permute-start | bytes 393224 | tf_op jit(solution)/shard_map/ppermute | solution.py:64
  146.2 11.5 %collective-permute-start.14 = (bf16[128,512]{0,1:T(8,128)(2,1)S(1)}, bf16[128,512]{0,1:T(8,128)(2,1)S(1)}, u32[]{:S(2)}, u32[]{:S(2)}) collective-permute-start(bf16[128,512]{0,1:T(8,128)(2,1)S(1)} %collective-permute-done.13), channel_id=1, source_target_pairs={{0,2},{2,4},{4,6},{6,8},{8,10},{10,12},{12,14},{14,16},{16,18},{18... | collective-permute-start | bytes 393224 | tf_op jit(solution)/shard_map/ppermute | solution.py:64
  193.4 152.0 %all-gather.9.cloned.1.call-start = ((), (), s32[]{:S(2)}) async-start(), calls=%async_computation.5 | async-start | bytes 12255232 | tf_op jit(solution)/shard_map/all_gather | solution.py:106
  194.0 293.7 %all-gather.11.cloned.1.call-start = ((), (), s32[]{:S(2)}) async-start(), calls=%async_computation.6 | async-start | bytes 12255232 | tf_op jit(solution)/shard_map/all_gather | solution.py:101
  194.6 311.5 %reduce-scatter.5.cloned.1.call-start = ((), (), s32[]{:S(2)}) async-start(), calls=%async_computation.7 | async-start | bytes 786432 | tf_op jit(solution)/shard_map/reduce_scatter | solution.py:118
  204.9 149.7 %copy-start.9 = (f32[3,2816]{1,0:T(4,128)S(1)}, f32[3,2816]{1,0:T(4,128)}, u32[]{:S(2)}) copy-start(f32[3,2816]{1,0:T(4,128)} %param.26) | copy-start | bytes 101380
  351.4 4.6 collective-permute-start.15
  (12 other events, 96.9 us)
Sparse Core Ops, SparseCore 0:
  10.0 73.1 all-gather.4
  86.0 97.6 all-gather.6
  193.5 6.6 reduce-scatter.2
  202.9 142.5 all-gather.8
  348.1 139.5 all-gather.10
  500.0 6.0 reduce-scatter.4
